TPU v7x, 32 devices: a whole 2x2x4 slice. The times are simulated.
32 devices in a mesh: sp: 8 (over z, x), tp: 4 (over y, core).
Axes of the slice: x: 2, y: 2, z: 4, core: 2. Of those that a mesh axis runs over, the one named last changes fastest.
Arguments:
- queries: bfloat16 [5120, 2048], P('sp', 'tp'), may hold values from -164 to 164
- keys: bfloat16 [5120, 512], P('sp', 'tp'), may hold values from -6 to 6
- values: bfloat16 [5120, 512], P('sp', 'tp'), may hold values from -6 to 6
- sink: float32 [32], P('tp'), may hold values from 4 to 8
- stream: bfloat16 [5120, 2048], P(('sp', 'tp')), may hold values from -6 to 6
- out_weight: bfloat16 [2048, 2048], P('tp'), may hold values from -0.5390625 to 0.5390625
- norm_gain: float32 [2048], replicated, may hold values from 0.1 to 1.9
- gate_weight: bfloat16 [2048, 5632], P('sp', 'tp'), may hold values from -0.125 to 0.125
- up_weight: bfloat16 [2048, 5632], P('sp', 'tp'), may hold values from -0.125 to 0.125
- down_weight: bfloat16 [5632, 2048], P('tp', 'sp'), may hold values from -0.23925781 to 0.23925781
Outputs:
- result: bfloat16 [5120, 2048], P(('sp', 'tp'))
All inputs are finite; a program needn't handle non-finite values.
Results may differ from a plain program's by a relative error of at most 0.019.
Values may be sent and summed in bfloat16 or wider, within the bound.
A program may use at most 128 MiB of HBM per device.

v0:
```python
import jax
import jax.numpy as jnp
from jax import lax
from jax.sharding import PartitionSpec as P

HEAD = 64
WINDOW = 128


def padded_2(cells, sides, width):
    for axis, dim in sides:
        count = lax.axis_size(axis)
        ends = count - 1
        head = lax.slice_in_dim(cells, 0, width, axis=dim)
        tail = lax.slice_in_dim(cells, cells.shape[dim] - width, cells.shape[dim], axis=dim)
        cells = jnp.concatenate(
            [
                lax.ppermute(tail, axis, [(i, (i + 1) % count) for i in range(ends)]),
                cells,
                lax.ppermute(head, axis, [((i + 1) % count, i) for i in range(ends)]),
            ],
            axis=dim,
        )
    return cells


def rotary(block, start):
    length = block.shape[0]
    middle = HEAD // 2
    inverse = 1.0 / 10000.0 ** (jnp.arange(0, HEAD, 2, dtype=jnp.float32) / HEAD)
    places = (start + jnp.arange(length, dtype=jnp.int32)).astype(jnp.float32)
    angles = places[:, None, None] * inverse[None, None, :]
    cosine_table = jnp.cos(angles)
    sine_table = jnp.sin(angles)
    pieces = block.astype(jnp.float32).reshape(length, -1, HEAD)
    leading = pieces[..., :middle]
    trailing = pieces[..., middle:]
    turned = jnp.concatenate(
        [
            leading * cosine_table - trailing * sine_table,
            trailing * cosine_table + leading * sine_table,
        ],
        -1,
    )
    return turned.reshape(length, -1).astype(jnp.bfloat16)


def window_attend(queries, keys, values, sink):
    rows_here = queries.shape[0]
    start = lax.axis_index("sp") * rows_here
    length = lax.axis_size("sp") * rows_here
    blocks = rows_here // WINDOW
    kv_width = keys.shape[1]
    kv_count = kv_width // HEAD
    head_count = queries.shape[1] // HEAD
    group = head_count // kv_count
    turned_q = rotary(queries, start)
    turned_k = rotary(keys, start)
    paired = jnp.concatenate([turned_k, values], 1)
    padded = padded_2(paired, (("sp", 0),), WINDOW)
    framed = padded.reshape(blocks + 2, WINDOW, 2 * kv_width)
    banded = jnp.concatenate([framed[:-2], framed[1:-1], framed[2:]], axis=1)
    key_band = banded[..., :kv_width].reshape(blocks, 3 * WINDOW, kv_count, HEAD)
    value_band = banded[..., kv_width:].reshape(blocks, 3 * WINDOW, kv_count, HEAD)
    query_blocks = turned_q.reshape(blocks, WINDOW, kv_count, group, HEAD)
    scores = jnp.einsum(
        "nqkgd,nskd->nkgqs", query_blocks, key_band, preferred_element_type=jnp.float32
    ) * HEAD ** (-0.5)
    query_place = (
        start + jnp.arange(blocks)[:, None, None] * WINDOW + jnp.arange(WINDOW)[None, :, None]
    )
    key_place = (
        start
        + jnp.arange(blocks)[:, None, None] * WINDOW
        - WINDOW
        + jnp.arange(3 * WINDOW)[None, None, :]
    )
    valid = (jnp.abs(key_place - query_place) <= WINDOW) & (key_place >= 0) & (key_place < length)
    scores = jnp.where(valid[:, None, None], scores, -jnp.inf)
    sink_grid = sink.reshape(kv_count, group)[None, :, :, None]
    top = jnp.maximum(jnp.max(scores, -1), sink_grid)
    raised = jnp.exp(scores - top[..., None])
    denom = jnp.sum(raised, -1) + jnp.exp(sink_grid - top)
    weights = (raised / denom[..., None]).astype(jnp.bfloat16)
    output = jnp.einsum(
        "nkgqs,nskd->nqkgd", weights, value_band, preferred_element_type=jnp.float32
    )
    return output.astype(jnp.bfloat16).reshape(rows_here, head_count * HEAD)


def collect_weights(gate_weight, up_weight, down_weight):
    return (
        lax.all_gather(gate_weight, "sp", axis=0, tiled=True),
        lax.all_gather(up_weight, "sp", axis=0, tiled=True),
        lax.all_gather(down_weight, "sp", axis=1, tiled=True),
    )


def local(
    queries, keys, values, sink, stream, out_weight, norm_gain, gate_weight, up_weight, down_weight
):
    attended = window_attend(queries, keys, values, sink)
    gathered = collect_weights(gate_weight, up_weight, down_weight)
    gate_whole, up_whole, down_whole = gathered
    rows = attended
    projected = lax.psum_scatter(
        jnp.dot(rows, out_weight, preferred_element_type=jnp.float32),
        "tp",
        scatter_dimension=0,
        tiled=True,
    )
    mixed = (stream.astype(jnp.float32) + projected).astype(jnp.bfloat16)
    mixed_wide = mixed.astype(jnp.float32)
    scale = lax.rsqrt(jnp.mean(mixed_wide * mixed_wide, -1, keepdims=True) + 1e-06)
    normed = (mixed_wide * scale * norm_gain).astype(jnp.bfloat16)
    piece = lax.all_gather(normed, "tp", axis=0, tiled=True)
    gate = jnp.dot(piece, gate_whole, preferred_element_type=jnp.float32)
    upward = jnp.dot(piece, up_whole, preferred_element_type=jnp.float32)
    hidden = (jax.nn.silu(gate) * upward).astype(jnp.bfloat16)
    rows = hidden
    lowered = lax.psum_scatter(
        jnp.dot(rows, down_whole, preferred_element_type=jnp.float32).astype(jnp.bfloat16),
        "tp",
        scatter_dimension=0,
        tiled=True,
    ).astype(jnp.float32)
    return (mixed_wide + 0.5 * lowered).astype(jnp.bfloat16)


def solution(mesh):
    placed = (
        P("sp", "tp"),
        P("sp", "tp"),
        P("sp", "tp"),
        P("tp"),
        P(("sp", "tp"), None),
        P("tp", None),
        P(),
        P("sp", "tp"),
        P("sp", "tp"),
        P("tp", "sp"),
    )
    return jax.shard_map(
        local, mesh=mesh, in_specs=placed, out_specs=P(("sp", "tp"), None), check_vma=False
    )
```

profile of v0, /device:TPU:0, one launch (start us, length us, event | category | flops | bytes accessed | tf_op | source)
XLA Modules:
  0.0 420.8 jit_solution(13338107045309871906)
XLA Ops:
  10.9 5.5 %collective-permute-start = (bf16[128,256]{0,1:T(8,128)(2,1)}, bf16[128,256]{0,1:T(8,128)(2,1)}, u32[]{:S(2)}, u32[]{:S(2)}) collective-permute-start(bf16[128,256]{0,1:T(8,128)(2,1)} %get-tuple-element.16), channel_id=1, source_target_pairs={{0,4},{4,8},{8,12},{12,16},{16,20},{20,24},{24,28},{1,5},{5,9},{9,... | collective-permute-start | bytes 196616 | tf_op jit(solution)/shard_map/ppermute | solution.py:18
  16.4 1.3 collective-permute-start.1
  17.9 1.4 copy.31
  21.6 1.8 convert_element_type.55
  23.4 1.3 max.17
  24.8 2.1 pad_maximum_fusion.5
  26.8 1.9 copy.26
  28.7 1.9 copy.27
  30.6 1.9 copy.28
  34.9 2.0 copy.30
  36.9 2.3 fusion.1
  39.3 1.9 fusion
  42.6 5.4 %fusion.9 = bf16[5,128,2,4,64]{1,4,3,2,0:T(8,128)(2,1)S(1)} fusion(bf16[5,384,2,64,1]{1,3,4,2,0:T(8,128)(2,1)S(1)} %bitcast.59, f32[5,2,384,128,4]{3,2,4,1,0:T(8,128)} %copy-done.1, f32[5,2,4,128]{3,2,1,0:T(4,128)S(1)} %exponential_add_fusion, f32[5,2,4,128]{3,2,1,0:T(4,128)S(1)} %broadcast_maximum_fusion, pred[5,128,384]{1,2,0:T(8,128)(4,1)S(1)} %fusion.11), kind=kOutput, calls=%fused_computation.18 | convolution fusion | flops 261816320 | bytes 9297920 | tf_op jit(solution)/shard_map/nkgqs,nskd->nqkgd/dot_general | solution.py:85
  48.5 4.0 fusion.12
  53.2 53.3 %reduce-scatter.3.cloned.1.call-done = f32[160,2048]{1,0:T(8,128)} async-done(((f32[640,2048]{1,0:T(8,128)}), f32[160,2048]{1,0:T(8,128)}) %reduce-scatter.3.cloned.1.call-update) | async-done | bytes 1310736 | tf_op jit(solution)/shard_map/reduce_scatter | solution.py:106
  106.4 1.6 fusion.5
  110.7 39.1 %all-gather.7.cloned.1.call-done = bf16[2048,1408]{1,0:T(8,128)(2,1)} async-done(((bf16[256,1408]{1,0:T(8,128)(2,1)}), bf16[2048,1408]{1,0:T(8,128)(2,1)}) %all-gather.7.cloned.1.call-update) | async-done | bytes 5767184 | tf_op jit(solution)/shard_map/all_gather | solution.py:93
  149.8 25.0 %all-gather.5.cloned.1.call-done = bf16[640,2048]{1,0:T(8,128)(2,1)} async-done(((bf16[160,2048]{1,0:T(8,128)(2,1)}), bf16[640,2048]{1,0:T(8,128)(2,1)}) %all-gather.5.cloned.1.call-update) | async-done | bytes 2621456 | tf_op jit(solution)/shard_map/all_gather | solution.py:116
  174.8 9.4 %fusion.25 = f32[640,1408]{1,0:T(8,128)} fusion(bf16[640,2048]{1,0:T(8,128)(2,1)} %all-gather.5.cloned.1.call-done, bf16[2048,1408]{1,0:T(8,128)(2,1)} %all-gather.7.cloned.1.call-done), kind=kOutput, calls=%fused_computation.62 | convolution fusion | flops 3690987520 | bytes 11993088 | tf_op jit(solution)/shard_map/dot_general | solution.py:117
  184.2 85.4 %all-gather.11.cloned.1.call-done = bf16[1408,2048]{1,0:T(8,128)(2,1)} async-done(((bf16[1408,256]{1,0:T(8,128)(2,1)}), bf16[1408,2048]{1,0:T(8,128)(2,1)}) %all-gather.11.cloned.1.call-update) | async-done | bytes 5767184 | tf_op jit(solution)/shard_map/all_gather | solution.py:95
  269.6 92.5 %all-gather.9.cloned.1.call-done = bf16[2048,1408]{1,0:T(8,128)(2,1)} async-done(((bf16[256,1408]{1,0:T(8,128)(2,1)}), bf16[2048,1408]{1,0:T(8,128)(2,1)}) %all-gather.9.cloned.1.call-update) | async-done | bytes 5767184 | tf_op jit(solution)/shard_map/all_gather | solution.py:94
  362.1 16.1 %convolution_convert_fusion = bf16[640,2048]{1,0:T(8,128)(2,1)} fusion(bf16[1408,2048]{1,0:T(8,128)(2,1)} %all-gather.11.cloned.1.call-done, bf16[640,2048]{1,0:T(8,128)(2,1)} %all-gather.5.cloned.1.call-done, bf16[2048,1408]{1,0:T(8,128)(2,1)} %all-gather.9.cloned.1.call-done, f32[640,1408]{1,0:T(8,128)} %fusion.25), kind=kOutput, calls=%fused_computation.8 | convolution fusion | flops 7388692480 | bytes 20381696 | tf_op jit(solution)/shard_map/dot_general | solution.py:122
  378.3 32.8 %reduce-scatter.5.cloned.1.call-done = bf16[160,2048]{1,0:T(8,128)(2,1)} async-done(((bf16[640,2048]{1,0:T(8,128)(2,1)}), bf16[160,2048]{1,0:T(8,128)(2,1)}) %reduce-scatter.5.cloned.1.call-update) | async-done | bytes 655376 | tf_op jit(solution)/shard_map/reduce_scatter | solution.py:121
  411.1 2.1 fusion.8
  (53 shorter events, 13.7 us)
Async XLA Ops:
  7.4 41.2 %copy-start = (bf16[512,2048]{1,0:T(8,128)(2,1)S(1)}, bf16[512,2048]{1,0:T(8,128)(2,1)}, u32[]{:S(2)}) copy-start(bf16[512,2048]{1,0:T(8,128)(2,1)} %param.15) | copy-start | bytes 6291460
  7.4 99.1 %reduce-scatter.3.cloned.1.call-start = ((), (), s32[]{:S(2)}) async-start(), calls=%async_computation.2 | async-start | bytes 6553600 | tf_op jit(solution)/shard_map/reduce_scatter | solution.py:106
  10.2 7.6 %copy-start.3 = (bf16[640,2,64]{0,2,1:T(8,128)(2,1)}, bf16[640,2,64]{0,2,1:T(8,128)(2,1)S(1)}, u32[]{:S(2)}) copy-start(bf16[640,2,64]{0,2,1:T(8,128)(2,1)S(1)} %pad_maximum_fusion.7) | copy-start | bytes 491524
  10.9 13.9 %collective-permute-start = (bf16[128,256]{0,1:T(8,128)(2,1)}, bf16[128,256]{0,1:T(8,128)(2,1)}, u32[]{:S(2)}, u32[]{:S(2)}) collective-permute-start(bf16[128,256]{0,1:T(8,128)(2,1)} %get-tuple-element.16), channel_id=1, source_target_pairs={{0,4},{4,8},{8,12},{12,16},{16,20},{20,24},{24,28},{1,5},{5,9},{9,... | collective-permute-start | bytes 196616 | tf_op jit(solution)/shard_map/ppermute | solution.py:18
  16.4 8.4 %collective-permute-start.1 = (bf16[128,256]{0,1:T(8,128)(2,1)}, bf16[128,256]{0,1:T(8,128)(2,1)}, u32[]{:S(2)}, u32[]{:S(2)}) collective-permute-start(bf16[128,256]{0,1:T(8,128)(2,1)} %get-tuple-element.17), channel_id=1, source_target_pairs={{4,0},{8,4},{12,8},{16,12},{20,16},{24,20},{28,24},{5,1},{9,5},{13... | collective-permute-start | bytes 196616 | tf_op jit(solution)/shard_map/ppermute | solution.py:20
  36.9 2.3 copy-start.6
  39.2 3.1 copy-start.1
  39.3 3.0 copy-start.2
  52.5 53.9 %copy-start.4 = (bf16[160,2048]{1,0:T(8,128)(2,1)S(1)}, bf16[160,2048]{1,0:T(8,128)(2,1)}, u32[]{:S(2)}) copy-start(bf16[160,2048]{1,0:T(8,128)(2,1)} %param.14) | copy-start | bytes 1966084
  52.5 55.5 %copy-start.5 = (f32[2048]{0:T(1024)S(1)}, f32[2048]{0:T(1024)}, u32[]{:S(2)}) copy-start(f32[2048]{0:T(1024)} %param.16) | copy-start | bytes 24580
  52.5 97.2 %all-gather.7.cloned.1.call-start = ((), (), s32[]{:S(2)}) async-start(), calls=%async_computation.4 | async-start | bytes 6488064 | tf_op jit(solution)/shard_map/all_gather | solution.py:93
  53.1 121.7 %all-gather.5.cloned.1.call-start = ((), (), s32[]{:S(2)}) async-start(), calls=%async_computation.3 | async-start | bytes 3276800 | tf_op jit(solution)/shard_map/all_gather | solution.py:116
  109.1 160.5 %all-gather.11.cloned.1.call-start = ((), (), s32[]{:S(2)}) async-start(), calls=%async_computation.6 | async-start | bytes 6488064 | tf_op jit(solution)/shard_map/all_gather | solution.py:95
  109.7 252.4 %all-gather.9.cloned.1.call-start = ((), (), s32[]{:S(2)}) async-start(), calls=%async_computation.5 | async-start | bytes 6488064 | tf_op jit(solution)/shard_map/all_gather | solution.py:94
  110.4 300.6 %reduce-scatter.5.cloned.1.call-start = ((), (), s32[]{:S(2)}) async-start(), calls=%async_computation.7 | async-start | bytes 3276800 | tf_op jit(solution)/shard_map/reduce_scatter | solution.py:121
Sparse Core Ops, SparseCore 0:
  52.7 53.7 reduce-scatter.2
  378.4 32.6 reduce-scatter.4
Sparse Core Ops, SparseCore 1:
  55.2 94.5 all-gather.6
  151.2 23.5 all-gather.4
  176.7 92.8 all-gather.10
  271.8 90.3 all-gather.8
where the time goes:
time: 421 us
  waiting for transfers between devices  330 us (78%)
  matrix products  37.2 us (9%)
  local copies, waits for them, and re-layouts  17.4 us (4%)
  between operations  15.2 us (4%)
  other arithmetic  13.9 us (3%)
  starting transfers between devices  7.16 us (2%)
    all_gather x1, waiting for transfers between devices, collect_weights(): lax.all_gather(up_weight, 'sp', axis=0, tiled=True)  92.5 us
    all_gather x1, waiting for transfers between devices, collect_weights(): lax.all_gather(down_weight, 'sp', axis=1, tiled=True)  85.4 us
    reduce_scatter x1, waiting for transfers between devices, local(): lax.psum_scatter(jnp.dot(rows, out_weight, preferred_element_type=jnp.flo...  53.3 us
    all_gather x1, waiting for transfers between devices, collect_weights(): lax.all_gather(gate_weight, 'sp', axis=0, tiled=True)  39.1 us
    reduce_scatter x1, waiting for transfers between devices, local(): lax.psum_scatter(jnp.dot(rows, down_whole, preferred_element_type=jnp.flo...  32.8 us
    all_gather x1, waiting for transfers between devices, local(): piece = lax.all_gather(normed, 'tp', axis=0, tiled=True)  25 us
    dot_general x1, matrix products, local(): jnp.dot(rows, down_whole, preferred_element_type=jnp.float32)  16.1 us
    dot_general x1, matrix products, local(): gate = jnp.dot(piece, gate_whole, preferred_element_type=jnp.float32)  9.43 us
  transfers between devices with their start and end apart: 8, of which 6 were waited for; matrix products, arithmetic and copies ran while one was open for 5% of the time, Pallas kernels for 0%

commit v1 on v0

--- a/solution.py
+++ b/solution.py
@@ -5,6 +5,12 @@
 
 HEAD = 64
 WINDOW = 128
+
+
+def all_parts(block, axis, d):
+    shards = lax.all_gather(block, axis, axis=0, tiled=False)
+    whole = jnp.concatenate(shards, axis=d)
+    return whole
 
 
 def padded_2(cells, sides, width):
@@ -92,7 +98,7 @@
     return (
         lax.all_gather(gate_weight, "sp", axis=0, tiled=True),
         lax.all_gather(up_weight, "sp", axis=0, tiled=True),
-        lax.all_gather(down_weight, "sp", axis=1, tiled=True),
+        all_parts(down_weight, "sp", 1),
     )
 
 

time: 421 us -> 421 us (level)
  waiting for transfers between devices: 330 us -> 321 us
  local copies, waits for them, and re-layouts: 17.4 us -> 25.7 us
    all_gather x1, waiting for transfers between devices: 85.4 us -> 39.7 us  [all_parts(): shards = lax.all_gather(block, axis, axis=0, tiled=False)]
    all_gather x1, waiting for transfers between devices: 39.1 us -> 84.1 us  [collect_weights(): lax.all_gather(gate_weight, 'sp', axis=0, tiled=True)]
    reshape x0 -> x1, local copies, waits for them, and re-layouts: none -> 8.24 us  [all_parts(): whole = jnp.concatenate(shards, axis=d)]
    all_gather x1, waiting for transfers between devices: 92.5 us -> 84.9 us  [collect_weights(): lax.all_gather(up_weight, 'sp', axis=0, tiled=True)]
  transfers between devices with their start and end apart: 8 -> 8, of which waited for: 6 -> 6; matrix products, arithmetic and copies ran while one was open for 5% -> 7% of each run, Pallas kernels for 0% -> 0%
where the time goes in v1:
time: 421 us; the launch traced here: 420 us
  waiting for transfers between devices  321 us (76%)
  matrix products  37.4 us (9%)
  local copies, waits for them, and re-layouts  25.7 us (6%)
  between operations  15.2 us (4%)
  other arithmetic  13.9 us (3%)
  starting transfers between devices  7.15 us (2%)
    all_gather x1, waiting for transfers between devices, collect_weights(): lax.all_gather(up_weight, 'sp', axis=0, tiled=True)  84.9 us
    all_gather x1, waiting for transfers between devices, collect_weights(): lax.all_gather(gate_weight, 'sp', axis=0, tiled=True)  84.1 us
    reduce_scatter x1, waiting for transfers between devices, local(): lax.psum_scatter(jnp.dot(rows, out_weight, preferred_element_type=jnp.flo...  52.7 us
    all_gather x1, waiting for transfers between devices, all_parts(): shards = lax.all_gather(block, axis, axis=0, tiled=False)  39.7 us
    reduce_scatter x1, waiting for transfers between devices, local(): lax.psum_scatter(jnp.dot(rows, down_whole, preferred_element_type=jnp.flo...  32.8 us
    all_gather x1, waiting for transfers between devices, local(): piece = lax.all_gather(normed, 'tp', axis=0, tiled=True)  25 us
    dot_general x1, matrix products, local(): jnp.dot(rows, down_whole, preferred_element_type=jnp.float32)  16.2 us
    dot_general x1, matrix products, local(): gate = jnp.dot(piece, gate_whole, preferred_element_type=jnp.float32)  9.5 us
  transfers between devices with their start and end apart: 8, of which 6 were waited for; matrix products, arithmetic and copies ran while one was open for 7% of the time, Pallas kernels for 0%

profile of v1, /device:TPU:0, one launch (start us, length us, event | category | flops | bytes accessed | tf_op | source)
XLA Modules:
  0.0 420.3 jit_solution(14168148018029706920)
XLA Ops:
  10.9 5.5 %collective-permute-start = (bf16[128,256]{0,1:T(8,128)(2,1)}, bf16[128,256]{0,1:T(8,128)(2,1)}, u32[]{:S(2)}, u32[]{:S(2)}) collective-permute-start(bf16[128,256]{0,1:T(8,128)(2,1)} %get-tuple-element.16), channel_id=1, source_target_pairs={{0,4},{4,8},{8,12},{12,16},{16,20},{20,24},{24,28},{1,5},{5,9},{9,... | collective-permute-start | bytes 196616 | tf_op jit(solution)/shard_map/ppermute | solution.py:24
  17.9 1.4 copy.31
  21.6 1.8 convert_element_type.55
  23.4 1.3 max.17
  24.8 2.1 pad_maximum_fusion.5
  26.8 1.9 copy.26
  28.7 1.9 copy.27
  30.6 1.9 copy.28
  34.9 2.0 copy.30
  36.9 2.3 fusion.1
  39.3 1.9 fusion
  42.6 5.4 %fusion.9 = bf16[5,128,2,4,64]{1,4,3,2,0:T(8,128)(2,1)S(1)} fusion(bf16[5,384,2,64,1]{1,3,4,2,0:T(8,128)(2,1)S(1)} %bitcast.65, f32[5,2,384,128,4]{3,2,4,1,0:T(8,128)} %copy-done.2, f32[5,2,4,128]{3,2,1,0:T(4,128)S(1)} %exponential_add_fusion, f32[5,2,4,128]{3,2,1,0:T(4,128)S(1)} %broadcast_maximum_fusion, pred[5,128,384]{1,2,0:T(8,128)(4,1)S(1)} %fusion.11), kind=kOutput, calls=%fused_computation.18 | convolution fusion | flops 261816320 | bytes 9297920 | tf_op jit(solution)/shard_map/nkgqs,nskd->nqkgd/dot_general | solution.py:91
  48.6 3.9 fusion.12
  53.8 52.7 %reduce-scatter.3.cloned.1.call-done = f32[160,2048]{1,0:T(8,128)} async-done(((f32[640,2048]{1,0:T(8,128)}), f32[160,2048]{1,0:T(8,128)}) %reduce-scatter.3.cloned.1.call-update) | async-done | bytes 1310736 | tf_op jit(solution)/shard_map/reduce_scatter | solution.py:112
  106.5 1.6 fusion.5
  110.1 39.7 %all-gather.12.cloned.1.call-done = bf16[11264,256]{1,0:T(8,128)(2,1)} async-done(((bf16[1408,256]{1,0:T(8,128)(2,1)}), bf16[11264,256]{1,0:T(8,128)(2,1)}) %all-gather.12.cloned.1.call-update) | async-done | bytes 5767184 | tf_op jit(solution)/shard_map/all_gather | solution.py:11
  149.8 8.2 %copy.35 = bf16[1408,8,256]{0,2,1:T(8,128)(2,1)} copy(bf16[1408,8,256]{2,0,1:T(8,128)(2,1)} %bitcast.54) | data formatting | bytes 11534336 | tf_op jit(solution)/shard_map/reshape | solution.py:12
  158.0 84.1 %all-gather.8.cloned.1.call-done = bf16[2048,1408]{1,0:T(8,128)(2,1)} async-done(((bf16[256,1408]{1,0:T(8,128)(2,1)}), bf16[2048,1408]{1,0:T(8,128)(2,1)}) %all-gather.8.cloned.1.call-update) | async-done | bytes 5767184 | tf_op jit(solution)/shard_map/all_gather | solution.py:99
  242.1 25.0 %all-gather.6.cloned.1.call-done = bf16[640,2048]{1,0:T(8,128)(2,1)} async-done(((bf16[160,2048]{1,0:T(8,128)(2,1)}), bf16[640,2048]{1,0:T(8,128)(2,1)}) %all-gather.6.cloned.1.call-update) | async-done | bytes 2621456 | tf_op jit(solution)/shard_map/all_gather | solution.py:122
  267.1 9.5 %fusion.25 = f32[640,1408]{1,0:T(8,128)} fusion(bf16[640,2048]{1,0:T(8,128)(2,1)} %all-gather.6.cloned.1.call-done, bf16[2048,1408]{1,0:T(8,128)(2,1)} %all-gather.8.cloned.1.call-done), kind=kOutput, calls=%fused_computation.62 | convolution fusion | flops 3690987520 | bytes 11993088 | tf_op jit(solution)/shard_map/dot_general | solution.py:123
  276.6 84.9 %all-gather.10.cloned.1.call-done = bf16[2048,1408]{1,0:T(8,128)(2,1)} async-done(((bf16[256,1408]{1,0:T(8,128)(2,1)}), bf16[2048,1408]{1,0:T(8,128)(2,1)}) %all-gather.10.cloned.1.call-update) | async-done | bytes 5767184 | tf_op jit(solution)/shard_map/all_gather | solution.py:100
  361.5 16.2 %convolution_convert_fusion = bf16[640,2048]{1,0:T(8,128)(2,1)} fusion(bf16[1408,2048]{0,1:T(8,128)(2,1)} %bitcast.55, bf16[640,2048]{1,0:T(8,128)(2,1)} %all-gather.6.cloned.1.call-done, bf16[2048,1408]{1,0:T(8,128)(2,1)} %all-gather.10.cloned.1.call-done, f32[640,1408]{1,0:T(8,128)} %fusion.25), kind=kOutput, calls=%fused_computation.8 | convolution fusion | flops 7388692480 | bytes 20381696 | tf_op jit(solution)/shard_map/dot_general | solution.py:128
  377.7 32.8 %reduce-scatter.5.cloned.1.call-done = bf16[160,2048]{1,0:T(8,128)(2,1)} async-done(((bf16[640,2048]{1,0:T(8,128)(2,1)}), bf16[160,2048]{1,0:T(8,128)(2,1)}) %reduce-scatter.5.cloned.1.call-update) | async-done | bytes 655376 | tf_op jit(solution)/shard_map/reduce_scatter | solution.py:127
  410.5 2.1 fusion.8
  (56 shorter events, 15.0 us)
Async XLA Ops:
  7.4 41.2 %copy-start = (bf16[512,2048]{1,0:T(8,128)(2,1)S(1)}, bf16[512,2048]{1,0:T(8,128)(2,1)}, u32[]{:S(2)}) copy-start(bf16[512,2048]{1,0:T(8,128)(2,1)} %param.15) | copy-start | bytes 6291460
  7.4 99.1 %reduce-scatter.3.cloned.1.call-start = ((), (), s32[]{:S(2)}) async-start(), calls=%async_computation.2 | async-start | bytes 6553600 | tf_op jit(solution)/shard_map/reduce_scatter | solution.py:112
  10.2 7.6 %copy-start.4 = (bf16[640,2,64]{0,2,1:T(8,128)(2,1)}, bf16[640,2,64]{0,2,1:T(8,128)(2,1)S(1)}, u32[]{:S(2)}) copy-start(bf16[640,2,64]{0,2,1:T(8,128)(2,1)S(1)} %pad_maximum_fusion.7) | copy-start | bytes 491524
  10.9 13.9 %collective-permute-start = (bf16[128,256]{0,1:T(8,128)(2,1)}, bf16[128,256]{0,1:T(8,128)(2,1)}, u32[]{:S(2)}, u32[]{:S(2)}) collective-permute-start(bf16[128,256]{0,1:T(8,128)(2,1)} %get-tuple-element.16), channel_id=1, source_target_pairs={{0,4},{4,8},{8,12},{12,16},{16,20},{20,24},{24,28},{1,5},{5,9},{9,... | collective-permute-start | bytes 196616 | tf_op jit(solution)/shard_map/ppermute | solution.py:24
  16.4 8.4 %collective-permute-start.1 = (bf16[128,256]{0,1:T(8,128)(2,1)}, bf16[128,256]{0,1:T(8,128)(2,1)}, u32[]{:S(2)}, u32[]{:S(2)}) collective-permute-start(bf16[128,256]{0,1:T(8,128)(2,1)} %get-tuple-element.17), channel_id=1, source_target_pairs={{4,0},{8,4},{12,8},{16,12},{20,16},{24,20},{28,24},{5,1},{9,5},{13... | collective-permute-start | bytes 196616 | tf_op jit(solution)/shard_map/ppermute | solution.py:26
  36.9 2.3 copy-start.7
  39.2 3.1 copy-start.2
  39.3 3.0 copy-start.3
  52.5 54.0 %copy-start.5 = (bf16[160,2048]{1,0:T(8,128)(2,1)S(1)}, bf16[160,2048]{1,0:T(8,128)(2,1)}, u32[]{:S(2)}) copy-start(bf16[160,2048]{1,0:T(8,128)(2,1)} %param.14) | copy-start | bytes 1966084
  52.5 55.6 %copy-start.6 = (f32[2048]{0:T(1024)S(1)}, f32[2048]{0:T(1024)}, u32[]{:S(2)}) copy-start(f32[2048]{0:T(1024)} %param.16) | copy-start | bytes 24580
  52.5 97.2 %all-gather.12.cloned.1.call-start = ((), (), s32[]{:S(2)}) async-start(), calls=%async_computation.7 | async-start | bytes 6488064 | tf_op jit(solution)/shard_map/all_gather | solution.py:11
  53.1 189.0 %all-gather.8.cloned.1.call-start = ((), (), s32[]{:S(2)}) async-start(), calls=%async_computation.4 | async-start | bytes 6488064 | tf_op jit(solution)/shard_map/all_gather | solution.py:99
  53.7 213.4 %all-gather.6.cloned.1.call-start = ((), (), s32[]{:S(2)}) async-start(), calls=%async_computation.3 | async-start | bytes 3276800 | tf_op jit(solution)/shard_map/all_gather | solution.py:122
  109.2 252.3 %all-gather.10.cloned.1.call-start = ((), (), s32[]{:S(2)}) async-start(), calls=%async_computation.5 | async-start | bytes 6488064 | tf_op jit(solution)/shard_map/all_gather | solution.py:100
  109.9 300.6 %reduce-scatter.5.cloned.1.call-start = ((), (), s32[]{:S(2)}) async-start(), calls=%async_computation.6 | async-start | bytes 3276800 | tf_op jit(solution)/shard_map/reduce_scatter | solution.py:127
  361.5 51.2 %copy-start.1 = (bf16[512,2048]{1,0:T(8,128)(2,1)S(1)}, bf16[512,2048]{1,0:T(8,128)(2,1)}, u32[]{:S(2)}) copy-start(bf16[512,2048]{1,0:T(8,128)(2,1)} %param.15) | copy-start | bytes 6291460
Sparse Core Ops, SparseCore 0:
  52.7 53.7 reduce-scatter.2
  377.9 32.6 reduce-scatter.4
Sparse Core Ops, SparseCore 1:
  55.2 94.5 all-gather.11
  151.8 90.2 all-gather.7
  243.6 23.5 all-gather.5
  269.4 92.1 all-gather.9
